TPU v7x, 32 devices: a whole 2x2x4 slice. The times are simulated.
32 devices in a mesh: ep: 16 (over z, y, x), tp: 2 (over core).
Axes of the slice: x: 2, y: 2, z: 4, core: 2. Of those that a mesh axis runs over, the one named last changes fastest.
Arguments:
- residual: bfloat16 [256, 2048], P(('ep', 'tp')), may hold values from -6 to 6
- query_latent: bfloat16 [256, 8, 512], P(('ep', 'tp')), may hold values from -40 to 40
- query_rotary: bfloat16 [256, 8, 32], P(('ep', 'tp')), may hold values from -6 to 6
- latent_new: bfloat16 [256, 512], P(('ep', 'tp')), may hold values from -16 to 16
- rotary_new: bfloat16 [256, 32], P(('ep', 'tp')), may hold values from -6 to 6
- latent_cache: bfloat16 [256, 256, 512], P(('ep', 'tp')), may hold values from -16 to 16
- rotary_cache: bfloat16 [256, 256, 32], P(('ep', 'tp')), may hold values from -6 to 6
- lengths: int32 [256], P(('ep', 'tp')), may hold values from 32 to 256, as said below
- value_up: bfloat16 [512, 8, 64], replicated, may hold values from -1 to 1
- out_proj: bfloat16 [512, 2048], replicated, may hold values from -0.5 to 0.5
- attn_gain: bfloat16 [2048], replicated, may hold values from 0.099609375 to 1.8984375
- mix_gate: bfloat16 [2048], replicated, may hold values from -0.125 to 0.125
- dense_w_gate: bfloat16 [2048, 2048], P(None, 'ep'), may hold values from -0.125 to 0.125
- dense_w_up: bfloat16 [2048, 2048], P(None, 'ep'), may hold values from -0.125 to 0.125
- dense_w_down: bfloat16 [2048, 2048], P('ep'), may hold values from -0.5 to 0.5
- expert_ids: int32 [256, 6], P(('ep', 'tp')), may hold values from 0 to 15, all different within a row; in each aligned block of 16 rows (0 to 15, 16 to 31, ...) at most 12 rows name the same one
- expert_scores: float32 [256, 6], P(('ep', 'tp')), may hold values from 0.1 to 5
- expert_gate: bfloat16 [16, 2048, 512], P('ep', None, 'tp'), may hold values from -0.125 to 0.125
- expert_up: bfloat16 [16, 2048, 512], P('ep', None, 'tp'), may hold values from -0.125 to 0.125
- expert_down: bfloat16 [16, 512, 2048], P('ep', 'tp'), may hold values from -1 to 1
- out_gain: bfloat16 [2048], replicated, may hold values from 0.099609375 to 1.8984375
Outputs:
- layer_out: bfloat16 [256, 2048], P(('ep', 'tp'))
Inputs may be any that keep to these rules, and one draw needn't show every extreme that they name: `expert_ids`: within each aligned block of 16 rows (the sequences of one ep index) no expert is named by more than 12 rows, a bound that some block reaches; a row names 6 different experts. `lengths`: some sequence has exactly 256 cached positions.
All inputs are finite; a program needn't handle non-finite values.
Results may differ from a plain program's by a relative error of at most 0.018.
Values may be sent and summed in bfloat16 or wider, within the bound.
A program may use at most 128 MiB of HBM per device.

v0:
```python
import functools
import math

import jax
import jax.numpy as jnp
from jax import lax
from jax.experimental import pallas as pl
from jax.experimental.pallas import tpu as pltpu
from jax.sharding import PartitionSpec as P

NOPE = 64
ALPHA = 8.0**0.25
EPS = 1e-06
ROPE_BASE = 10000.0
F32 = jnp.float32
BF16 = jnp.bfloat16
MESH = pl.DeviceIdType.MESH
VMEM = pltpu.VMEM


def normalize(values, gain):
    center = jnp.mean(values, -1, keepdims=True)
    shifted = values - center
    spread = jnp.mean(jnp.square(shifted), -1, keepdims=True)
    return shifted * lax.rsqrt(spread + EPS) * gain


def vector(ref):
    return ref[...].astype(F32).reshape(1, ref.shape[0])


def inner_size(n):
    size = 1
    while size * size < n:
        size *= 2
    return size if n % size == 0 else n


def silu(value):
    return value / (1.0 + jnp.exp(-value))


def dot(a, b):
    return jnp.dot(a, b, preferred_element_type=F32)


def dot_nt(a, b):
    return lax.dot_general(a, b, (((1,), (1,)), ((), ())), preferred_element_type=F32)


def kernel(
    n,
    lengths,
    residual,
    query_latent,
    query_rotary,
    latent_new,
    rotary_new,
    attn_gain,
    mix_gate,
    out_gain,
    ids,
    route_scores,
    rotary_cache,
    cache_hbm,
    vu_hbm,
    op_hbm,
    eg_hbm,
    eu_hbm,
    dg_hbm,
    du_hbm,
    ed_hbm,
    dd_hbm,
    out,
    cache,
    vu,
    op,
    eg,
    eu,
    dg,
    du,
    ed,
    dd,
    lat,
    gath,
    pout,
    pin,
    sbuf,
    rbuf,
    zbuf,
    hid_own,
    hid_other,
    hid_dense,
    cache_sem,
    w_sem,
    ag_send,
    ag_recv,
    fw_send,
    fw_recv,
    p_send,
    p_recv,
    rs_send,
    rs_recv,
):
    me = lax.axis_index("ep")
    core = lax.axis_index("tp")
    other = 1 - core
    seqs, width = residual.shape
    heads = query_latent.shape[1]
    rope = query_rotary.shape[-1]
    cache_len = cache.shape[1]
    extra = gath.shape[-1] - width
    experts = n

    cache_copies = [
        pltpu.make_async_copy(cache_hbm.at[s], cache.at[s], cache_sem.at[s]) for s in range(seqs)
    ]
    for c in cache_copies:
        c.start()
    pairs = [
        (vu_hbm, vu),
        (op_hbm, op),
        (eg_hbm.at[0], eg),
        (eu_hbm.at[0], eu),
        (dg_hbm, dg),
        (du_hbm, du),
        (ed_hbm.at[0], ed),
        (dd_hbm, dd),
    ]
    w_copies = [pltpu.make_async_copy(a, b, w_sem.at[k]) for k, (a, b) in enumerate(pairs)]
    for c in w_copies:
        c.start()

    barrier = pltpu.get_barrier_semaphore()

    inner = inner_size(n)
    outer = n // inner
    zo = lax.div(me, inner)
    xi = lax.rem(me, inner)

    def ahead(dz, dx):
        return lax.rem(zo + dz, outer) * inner + lax.rem(xi + dx, inner)

    def behind(dz, dx):
        return ahead(outer - dz, inner - dx)

    def greet_outer(d, carry):
        pl.semaphore_signal(barrier, inc=1, device_id={"ep": ahead(d, 0)}, device_id_type=MESH)
        return carry

    def greet_inner(d, carry):
        pl.semaphore_signal(barrier, inc=1, device_id={"ep": ahead(0, d)}, device_id_type=MESH)
        return carry

    lax.fori_loop(1, outer, greet_outer, 0)
    lax.fori_loop(1, inner, greet_inner, 0)
    pl.semaphore_signal(barrier, inc=1, device_id={"tp": other}, device_id_type=MESH)

    half = rope // 2
    lane = lax.broadcasted_iota(jnp.int32, (seqs, rope), 1)
    row = lax.broadcasted_iota(jnp.int32, (seqs, rope), 0)
    pos = jnp.zeros((seqs, rope), F32)
    for s in range(seqs):
        pos = jnp.where(row == s, lengths[s].astype(F32), pos)
    inv_freq = jnp.exp(lax.rem(lane, half).astype(F32) * (-math.log(ROPE_BASE) / half))
    angles = pos * inv_freq
    cosine = jnp.cos(angles)
    sine = jnp.sin(angles)
    ra = lax.broadcasted_iota(jnp.int32, (rope, rope), 0)
    rb = lax.broadcasted_iota(jnp.int32, (rope, rope), 1)
    swap = jnp.where(ra + half == rb, 1.0, jnp.where(ra == rb + half, -1.0, 0.0)).astype(BF16)
    q_rot = query_rotary[...].astype(F32).reshape(seqs * heads, rope)
    q_swap = dot(q_rot.astype(BF16), swap).reshape(seqs, heads, rope)
    q_rot = q_rot.reshape(seqs, heads, rope)
    k_rot = rotary_new[...]
    k_turn = (k_rot.astype(F32) * cosine + dot(k_rot, swap) * sine).astype(BF16).astype(F32)
    ln_all = latent_new[...].astype(F32)
    score_scale = (NOPE + rope) ** (-0.5)
    t_idx = lax.broadcasted_iota(jnp.int32, (heads, cache_len), 1)

    score_rows, own_rows_all = [], []
    for s in range(seqs):
        q_turn = (q_rot[s] * cosine[s : s + 1] + q_swap[s] * sine[s : s + 1]).astype(BF16)
        ql = query_latent[s]
        own_rows_all.append(
            jnp.sum(ql.astype(F32) * ln_all[s : s + 1], -1, keepdims=True)
            + jnp.sum(q_turn.astype(F32) * k_turn[s : s + 1], -1, keepdims=True)
        )
        rot_part = dot(q_turn, rotary_cache[s])
        cache_copies[s].wait()
        part = dot_nt(ql, cache[s]) + rot_part
        score_rows.append(jnp.where(t_idx < lengths[s], part, -jnp.inf))
    own = jnp.concatenate(own_rows_all, 0) * score_scale
    scores = jnp.concatenate(score_rows, 0) * score_scale
    top = jnp.maximum(jnp.max(scores, -1, keepdims=True), own)
    probs = jnp.exp(scores - top)
    own_p = jnp.exp(own - top)
    total = jnp.sum(probs, -1, keepdims=True) + own_p
    weights = probs / total
    own_w = (own_p / total).astype(BF16).astype(F32)
    for s in range(seqs):
        at = slice(s * heads, (s + 1) * heads)
        lat[at, :] = dot(weights[at].astype(BF16), cache[s]) + own_w[at] * ln_all[s : s + 1]

    w_copies[0].wait()
    w_copies[1].wait()
    wide = dot_nt(lat[...].astype(BF16), vu[...])
    vdim = wide.shape[1] // heads
    wide = wide.reshape(seqs, heads, wide.shape[1])
    h_row = lax.broadcasted_iota(jnp.int32, wide.shape, 1)
    h_lane = lax.broadcasted_iota(jnp.int32, wide.shape, 2)
    own_head = (h_lane >= h_row * vdim) & (h_lane < (h_row + 1) * vdim)
    heads_out = jnp.sum(jnp.where(own_head, wide, 0.0), 1).astype(BF16)
    attn = dot(heads_out, op[...]).astype(BF16).astype(F32)
    mixed = normalize(ALPHA * residual[...].astype(F32) + attn, vector(attn_gain)).astype(BF16)
    mixed_f = mixed.astype(F32)
    mix = 1.0 / (1.0 + jnp.exp(-jnp.sum(mixed_f * vector(mix_gate), -1, keepdims=True)))

    sc = route_scores[...]
    share = sc / jnp.sum(sc, -1, keepdims=True)
    e_lane = lax.broadcasted_iota(jnp.int32, (seqs, extra), 1)
    low = e_lane > experts
    e_idx = jnp.where(low, e_lane - (experts + 1), e_lane)
    coef = jnp.where(e_idx == experts, mix, 0.0)
    for k in range(ids.shape[1]):
        coef = coef + jnp.where(e_idx == ids[:, k : k + 1], share[:, k : k + 1], 0.0)
    high = coef.astype(BF16)
    coef = jnp.where(low, coef - high.astype(F32), high.astype(F32)).astype(BF16)
    mine = gath.at[core, me]
    mine[:, :width] = mixed
    mine[:, width:] = coef

    pl.semaphore_wait(barrier, outer + inner - 1)

    def ag_copy(slot, block, target):
        return pltpu.make_async_remote_copy(
            src_ref=gath.at[core, block],
            dst_ref=gath.at[core, block],
            send_sem=ag_send.at[slot],
            recv_sem=ag_recv.at[slot],
            device_id={"ep": target},
            device_id_type=MESH,
        )

    def fw_copy(d, half_idx, block):
        return pltpu.make_async_remote_copy(
            src_ref=gath.at[half_idx, block],
            dst_ref=gath.at[half_idx, block],
            send_sem=fw_send.at[d],
            recv_sem=fw_recv.at[d],
            device_id={"tp": other},
            device_id_type=MESH,
        )

    def ag_outer(d, carry):
        ag_copy(d * inner, me, ahead(d, 0)).start()
        return carry

    def ag_inner(dz, block):
        def send(d, carry):
            ag_copy(dz * inner + d, block, ahead(0, d)).start()
            return carry

        lax.fori_loop(1, inner, send, 0)

    lax.fori_loop(1, outer, ag_outer, 0)
    ag_inner(0, me)
    fw_copy(0, core, me).start()

    def ag_relay(dz, carry):
        block = behind(dz, 0)
        ag_copy(dz * inner, block, me).wait_recv()
        ag_inner(dz, block)
        fw_copy(dz * inner, core, block).start()
        return carry

    lax.fori_loop(1, outer, ag_relay, 0)

    def ag_forward(dz, carry):
        def one(dx, inside):
            block = behind(dz, dx)
            ag_copy(dz * inner + dx, block, me).wait_recv()
            fw_copy(dz * inner + dx, core, block).start()
            return inside

        return lax.fori_loop(1, inner, one, carry)

    lax.fori_loop(0, outer, ag_forward, 0)
    for c in w_copies[2:6]:
        c.wait()

    chunk = min(n, 16)
    rows = chunk * seqs

    def load(half_idx, b):
        block = gath[half_idx, pl.ds(b * chunk, chunk)]
        flat = block.astype(F32).reshape(rows, width + extra)
        x = flat[:, :width].astype(BF16)
        tail = flat[:, width:]
        c_lane = lax.broadcasted_iota(jnp.int32, (rows, extra), 1)
        pick = (c_lane == me) | (c_lane == me + experts + 1)
        weight = jnp.sum(jnp.where(pick, tail, 0.0), -1, keepdims=True)
        pick = (c_lane == experts) | (c_lane == 2 * experts + 1)
        blend = jnp.sum(jnp.where(pick, tail, 0.0), -1, keepdims=True)
        return x, weight, blend

    def expert_hidden(x, weight):
        return (silu(dot(x, eg[...])) * dot(x, eu[...]) * weight).astype(BF16)

    def own_hidden(b, carry):
        x, weight, blend = load(core, b)
        at = pl.ds(b * rows, rows)
        hid_own[at, :] = expert_hidden(x, weight)
        hid_dense[at, :] = (silu(dot(x, dg[...])) * dot(x, du[...]) * blend).astype(BF16)
        return carry

    lax.fori_loop(0, n // chunk, own_hidden, 0)

    def fw_wait(d, carry):
        fw_copy(d, other, behind(lax.div(d, inner), lax.rem(d, inner))).wait_recv()
        return carry

    lax.fori_loop(0, n, fw_wait, 0)

    def partner_hidden(b, carry):
        x, weight, _ = load(other, b)
        hid_other[pl.ds(b * rows, rows), :] = expert_hidden(x, weight)
        return carry

    lax.fori_loop(0, n // chunk, partner_hidden, 0)
    for c in w_copies[6:]:
        c.wait()
    tiles, tile = sbuf.shape[0], sbuf.shape[-1]

    def p_copy(t):
        return pltpu.make_async_remote_copy(
            src_ref=pout.at[t],
            dst_ref=pin.at[t],
            send_sem=p_send.at[t],
            recv_sem=p_recv.at[t],
            device_id={"tp": other},
            device_id_type=MESH,
        )

    def rs_inner(t, slot, block, target):
        return pltpu.make_async_remote_copy(
            src_ref=sbuf.at[t, block],
            dst_ref=rbuf.at[t, slot],
            send_sem=rs_send.at[t, slot],
            recv_sem=rs_recv.at[t, slot],
            device_id={"ep": target},
            device_id_type=MESH,
        )

    def rs_outer(t, d, target):
        return pltpu.make_async_remote_copy(
            src_ref=zbuf.at[t, d],
            dst_ref=rbuf.at[t, d * inner],
            send_sem=rs_send.at[t, d * inner],
            recv_sem=rs_recv.at[t, d * inner],
            device_id={"ep": target},
            device_id_type=MESH,
        )

    for t in range(tiles):
        cols = slice(t * tile, (t + 1) * tile)

        def partner_rows(b, carry):
            part = dot(hid_other[pl.ds(b * rows, rows), :], ed[:, cols])
            pout[t, pl.ds(b * chunk, chunk)] = part.reshape(chunk, seqs, tile).astype(BF16)
            return carry

        lax.fori_loop(0, n // chunk, partner_rows, 0)
        p_copy(t).start()

    for t in range(tiles):
        cols = slice(t * tile, (t + 1) * tile)
        p_copy(t).wait_recv()

        def own_rows(b, carry):
            at = pl.ds(b * rows, rows)
            part = dot(hid_own[at, :], ed[:, cols]) + dot(hid_dense[at, :], dd[:, cols])
            part = part.reshape(chunk, seqs, tile)
            part = part + pin[t, pl.ds(b * chunk, chunk)].astype(F32)
            sbuf[t, pl.ds(b * chunk, chunk)] = part.astype(BF16)
            return carry

        lax.fori_loop(0, n // chunk, own_rows, 0)

        def rs_start(k, carry):
            dz = outer - 1 - k

            def one(dx, inside):
                rs_inner(t, dz * inner + dx, ahead(dz, dx), ahead(0, dx)).start()
                return inside

            return lax.fori_loop(1, inner, one, carry)

        lax.fori_loop(0, outer, rs_start, 0)

    def inner_sum(t, dz, start):
        def one(dx, total):
            rs_inner(t, dz * inner + dx, me, me).wait_recv()
            return total + rbuf[t, dz * inner + dx].astype(F32)

        return lax.fori_loop(1, inner, one, start)

    for t in range(tiles):

        def rs_relay(k, carry):
            dz = outer - k
            value = inner_sum(t, dz, sbuf[t, ahead(dz, 0)].astype(F32))
            zbuf[t, dz] = value.astype(BF16)
            rs_outer(t, dz, ahead(dz, 0)).start()
            return carry

        lax.fori_loop(1, outer, rs_relay, 0)

    sums = []
    for t in range(tiles):
        cols = slice(t * tile, (t + 1) * tile)
        start = ALPHA * mixed_f[:, cols] + sbuf[t, me].astype(F32)
        value = inner_sum(t, 0, start)

        def outer_add(d, total):
            rs_outer(t, d, me).wait_recv()
            return total + rbuf[t, d * inner].astype(F32)

        sums.append(lax.fori_loop(1, outer, outer_add, value))
    total = jnp.concatenate(sums, axis=-1)
    out[...] = normalize(total, vector(out_gain)).astype(BF16)

    def drain(d, carry):
        ag_copy(d, me, me).wait_send()
        for t in range(tiles):
            rs_inner(t, d, me, me).wait_send()
        return carry

    def drain_fw(d, carry):
        fw_copy(d, core, me).wait_send()
        return carry

    lax.fori_loop(1, n, drain, 0)
    lax.fori_loop(0, n, drain_fw, 0)
    for t in range(tiles):
        p_copy(t).wait_send()


def on_device(
    n,
    residual,
    query_latent,
    query_rotary,
    latent_new,
    rotary_new,
    latent_cache,
    rotary_cache,
    lengths,
    value_up,
    out_proj,
    attn_gain,
    mix_gate,
    dense_w_gate,
    dense_w_up,
    dense_w_down,
    expert_ids,
    expert_scores,
    expert_gate,
    expert_up,
    expert_down,
    out_gain,
):
    seqs, width = residual.shape
    heads = query_latent.shape[1]
    vu = value_up.transpose(1, 2, 0).reshape(-1, value_up.shape[0])
    rotary_turned = rotary_cache.transpose(0, 2, 1)
    extra = -(-2 * (n + 1) // 128) * 128
    vmem = pl.BlockSpec(memory_space=VMEM)
    hbm = pl.BlockSpec(memory_space=pl.ANY)
    smem = pl.BlockSpec(memory_space=pltpu.SMEM)
    dma = pltpu.SemaphoreType.DMA
    tile = 512 if width % 512 == 0 else width
    tiles = width // tile
    block = (tiles, n, seqs, tile)
    return pl.pallas_call(
        functools.partial(kernel, n),
        out_shape=jax.ShapeDtypeStruct((seqs, width), BF16),
        in_specs=[smem] + [vmem] * 11 + [hbm] * 9,
        out_specs=vmem,
        scratch_shapes=[
            VMEM(latent_cache.shape, BF16),
            VMEM(vu.shape, BF16),
            VMEM(out_proj.shape, BF16),
            VMEM(expert_gate.shape[1:], BF16),
            VMEM(expert_up.shape[1:], BF16),
            VMEM(dense_w_gate.shape, BF16),
            VMEM(dense_w_up.shape, BF16),
            VMEM(expert_down.shape[1:], BF16),
            VMEM(dense_w_down.shape, BF16),
            VMEM((seqs * heads, latent_cache.shape[-1]), F32),
            VMEM((2, n, seqs, width + extra), BF16),
            VMEM(block, BF16),
            VMEM(block, BF16),
            VMEM(block, BF16),
            VMEM(block, BF16),
            VMEM((tiles, n // inner_size(n), seqs, tile), BF16),
            VMEM((n * seqs, expert_gate.shape[-1]), BF16),
            VMEM((n * seqs, expert_gate.shape[-1]), BF16),
            VMEM((n * seqs, dense_w_gate.shape[-1]), BF16),
            dma((seqs,)),
            dma((8,)),
            dma((n,)),
            dma((n,)),
            dma((n,)),
            dma((n,)),
            dma((tiles,)),
            dma((tiles,)),
            dma((tiles, n)),
            dma((tiles, n)),
        ],
        compiler_params=pltpu.CompilerParams(
            collective_id=0, has_side_effects=True, vmem_limit_bytes=60 * 1024 * 1024
        ),
    )(
        lengths,
        residual,
        query_latent,
        query_rotary,
        latent_new,
        rotary_new,
        attn_gain,
        mix_gate,
        out_gain,
        expert_ids,
        expert_scores,
        rotary_turned,
        latent_cache,
        vu,
        out_proj,
        expert_gate,
        expert_up,
        dense_w_gate,
        dense_w_up,
        expert_down,
        dense_w_down,
    )


def solution(mesh):
    rows = P(("ep", "tp"), None)
    rows3 = P(("ep", "tp"), None, None)
    return jax.shard_map(
        functools.partial(on_device, mesh.shape["ep"]),
        mesh=mesh,
        in_specs=(
            rows,
            rows3,
            rows3,
            rows,
            rows,
            rows3,
            rows3,
            P(("ep", "tp")),
            P(),
            P(),
            P(),
            P(),
            P(None, "ep"),
            P(None, "ep"),
            P("ep", None),
            rows,
            rows,
            P("ep", None, "tp"),
            P("ep", None, "tp"),
            P("ep", "tp", None),
            P(),
        ),
        out_specs=rows,
        check_vma=False,
    )
```

profile of v0, /device:TPU:0, one launch (start us, length us, event | category | flops | bytes accessed | tf_op | source)
XLA Modules:
  0.0 37.7 jit_solution(3475972657205895654)
XLA Ops:
  0.0 36.3 %shard_map.199 = bf16[8,2048]{1,0:T(8,128)(2,1)} custom-call(s32[8]{0:T(128)} %lengths.1, bf16[8,2048]{1,0:T(8,128)(2,1)} %residual.1, bf16[8,8,512]{2,1,0:T(8,128)(2,1)} %query_latent.1, bf16[8,8,32]{2,1,0:T(8,128)(2,1)} %query_rotary.1, bf16[8,512]{1,0:T(8,128)(2,1)} %latent_new.1, bf16[8,32]{1,0:T(8,128)(2,1)} %rotary_new.1, bf16[2048]{0:T(1024)(128)(2,1)} %attn_gain.1, ...), custom_call_target="tpu_custom_call" | custom-call | tf_op jit(solution)/shard_map/pallas_call | solution.py:485
  36.3 1.4 %copy.23 = bf16[8,2048]{1,0:T(8,128)(2,1)} copy(bf16[8,2048]{1,0:T(8,128)(2,1)} %shard_map.199) | data formatting | bytes 65536
where the time goes:
time: 37.9 us; the launch traced here: 37.7 us
  Pallas kernels  36.3 us (96%)
  local copies, waits for them, and re-layouts  1.38 us (4%)
    pallas_call x1, Pallas kernels, on_device(): pl.pallas_call(functools.partial(kernel, n), out_shape=jax.ShapeDtypeStru...  36.3 us
    unnamed x1, local copies, waits for them, and re-layouts  1.38 us

commit v1 on v0

v1 whole, which is shorter than its diff:
```python
import functools
import math

import jax
import jax.numpy as jnp
from jax import lax
from jax.experimental import pallas as pl
from jax.experimental.pallas import tpu as pltpu
from jax.sharding import PartitionSpec as P

NOPE = 64
ALPHA = 8.0**0.25
EPS = 1e-06
ROPE_BASE = 10000.0
F32 = jnp.float32
BF16 = jnp.bfloat16
MESH = pl.DeviceIdType.MESH
VMEM = pltpu.VMEM


def inner_size(n):
    size = 1
    while size * size < n:
        size *= 2
    return size if n % size == 0 else n


def silu(value):
    return value / (1.0 + jnp.exp(-value))


def dot(a, b):
    return jnp.dot(a, b, preferred_element_type=F32)


def dot_nt(a, b):
    return lax.dot_general(a, b, (((1,), (1,)), ((), ())), preferred_element_type=F32)


def row_sum(value):
    return jnp.sum(value, -1, keepdims=True)


def kernel(
    n,
    group,
    lengths,
    qr_hbm,
    rn_hbm,
    ql_hbm,
    ln_hbm,
    rc_hbm,
    cache_hbm,
    res_hbm,
    ids_hbm,
    rs_hbm,
    vu_hbm,
    op_hbm,
    ag_hbm,
    mg_hbm,
    eg_hbm,
    eu_hbm,
    ed_hbm,
    dg_hbm,
    du_hbm,
    dd_hbm,
    og_hbm,
    out,
    query_rotary,
    rotary_new,
    query_latent,
    latent_new,
    rotary_cache,
    cache,
    ids,
    route_scores,
    vu,
    op,
    attn_gain,
    mix_gate,
    eg,
    eu,
    down,
    dg,
    du,
    out_gain,
    lat,
    rows_all,
    heads_all,
    wide_rows,
    mixed,
    scale,
    hid,
    sbuf,
    rbuf,
    zbuf,
    zrecv,
    in_sem,
    cache_sem,
    w_send,
    w_recv,
    r_send,
    r_line,
    r_plane,
    h_send,
    h_recv,
    s_send,
    s_plane,
    s_line,
):
    me = lax.axis_index("ep")
    core = lax.axis_index("tp")
    other = 1 - core
    seqs, heads, kl = query_latent.shape
    rope = query_rotary.shape[-1]
    cache_len = cache.shape[1]
    width = res_hbm.shape[1]
    extra = rows_all.shape[-1] - width
    half_fe = eg.shape[-1]
    fd = dg.shape[-1]
    inner = inner_size(n)
    outer = n // inner
    plane_rows = inner * seqs
    zo = lax.div(me, inner)
    xi = lax.rem(me, inner)
    upper = lax.div(2 * zo, outer)

    def far(k):
        down_order = outer - 1 - k
        down_order = down_order - jnp.where(down_order <= zo, 1, 0)
        up_order = k + jnp.where(zo <= k, 1, 0)
        return down_order + upper * (up_order - down_order)

    others = [far(k) for k in range(outer - 1)]

    def mate(d):
        return zo * inner + lax.rem(xi + d, inner)

    barrier = pltpu.get_barrier_semaphore()

    def greet(d, carry):
        peer = lax.rem(me + d, n)
        pl.semaphore_signal(barrier, inc=1, device_id={"ep": peer}, device_id_type=MESH)
        return carry

    lax.fori_loop(1, n, greet, 0)
    pl.semaphore_signal(barrier, inc=1, device_id={"tp": other}, device_id_type=MESH)

    own_down = down.at[pl.ds(pl.multiple_of(core * half_fe, half_fe), half_fe)]
    names = {}

    def load(name, a, b):
        c = pltpu.make_async_copy(a, b, in_sem.at[len(names)])
        c.start()
        names[name] = c

    load("qr", qr_hbm, query_rotary)
    load("rn", rn_hbm, rotary_new)
    load("ql", ql_hbm, query_latent)
    load("ln", ln_hbm, latent_new)
    load("rc", rc_hbm, rotary_cache)
    cache_copies = [
        pltpu.make_async_copy(cache_hbm.at[s], cache.at[s], cache_sem.at[s]) for s in range(seqs)
    ]
    for c in cache_copies:
        c.start()
    load("res", res_hbm, rows_all.at[me, :, pl.ds(0, width)])
    load("ids", ids_hbm, ids)
    load("rs", rs_hbm, route_scores)
    load("vu", vu_hbm, vu)
    load("op", op_hbm, op)
    load("ag", ag_hbm, attn_gain)
    load("mg", mg_hbm, mix_gate)
    load("eg", eg_hbm.at[0], eg.at[core])
    load("eu", eu_hbm.at[0], eu.at[core])
    load("ed", ed_hbm.at[0], own_down)
    load("dg", dg_hbm, dg)
    load("du", du_hbm, du)
    load("dd", dd_hbm, down.at[pl.ds(2 * half_fe, fd)])
    load("og", og_hbm, out_gain)

    half = rope // 2
    lane = lax.broadcasted_iota(jnp.int32, (seqs, rope), 1)
    row = lax.broadcasted_iota(jnp.int32, (seqs, rope), 0)
    pos = jnp.zeros((seqs, rope), F32)
    for s in range(seqs):
        pos = jnp.where(row == s, lengths[s].astype(F32), pos)
    inv_freq = jnp.exp(lax.rem(lane, half).astype(F32) * (-math.log(ROPE_BASE) / half))
    angles = pos * inv_freq
    cosine = jnp.cos(angles)
    sine = jnp.sin(angles)
    ra = lax.broadcasted_iota(jnp.int32, (rope, rope), 0)
    rb = lax.broadcasted_iota(jnp.int32, (rope, rope), 1)
    swap = jnp.where(ra + half == rb, 1.0, jnp.where(ra == rb + half, -1.0, 0.0)).astype(BF16)
    for name in ("qr", "rn", "ql", "ln", "rc"):
        names[name].wait()
    q_rot = query_rotary[...].astype(F32).reshape(seqs * heads, rope)
    q_swap = dot(q_rot.astype(BF16), swap).reshape(seqs, heads, rope)
    q_rot = q_rot.reshape(seqs, heads, rope)
    k_rot = rotary_new[...]
    k_turn = (k_rot.astype(F32) * cosine + dot(k_rot, swap) * sine).astype(BF16).astype(F32)
    ln_all = latent_new[...].astype(F32)
    score_scale = (NOPE + rope) ** (-0.5)
    t_idx = lax.broadcasted_iota(jnp.int32, (heads, cache_len), 1)

    score_rows, own_rows_all = [], []
    for s in range(seqs):
        q_turn = (q_rot[s] * cosine[s : s + 1] + q_swap[s] * sine[s : s + 1]).astype(BF16)
        ql = query_latent[s]
        own_rows_all.append(
            row_sum(ql.astype(F32) * ln_all[s : s + 1])
            + row_sum(q_turn.astype(F32) * k_turn[s : s + 1])
        )
        rot_part = dot(q_turn, rotary_cache[s])
        cache_copies[s].wait()
        part = dot_nt(ql, cache[s]) + rot_part
        score_rows.append(jnp.where(t_idx < lengths[s], part, -jnp.inf))
    own = jnp.concatenate(own_rows_all, 0) * score_scale
    scores = jnp.concatenate(score_rows, 0) * score_scale

    names["ids"].wait()
    names["rs"].wait()
    sc = route_scores[...]
    share = sc / row_sum(sc)
    e_lane = lax.broadcasted_iota(jnp.int32, (seqs, extra), 1)
    low = e_lane >= n
    e_idx = jnp.where(low, e_lane - n, e_lane)
    coef = jnp.zeros((seqs, extra), F32)
    for k in range(ids.shape[1]):
        coef = coef + jnp.where(e_idx == ids[:, k : k + 1], share[:, k : k + 1], 0.0)
    high = coef.astype(BF16)
    coef = jnp.where(low, coef - high.astype(F32), high.astype(F32)).astype(BF16)
    rows_all[me, :, width:] = coef

    pl.semaphore_wait(barrier, n)

    def row_copy(block, sem, target):
        return pltpu.make_async_remote_copy(
            src_ref=rows_all.at[block],
            dst_ref=rows_all.at[block],
            send_sem=r_send,
            recv_sem=sem,
            device_id={"ep": target},
            device_id_type=MESH,
        )

    def to_plane(p):
        block = p * inner + xi

        def send(d, carry):
            row_copy(block, r_plane.at[p], mate(d)).start()
            return carry

        lax.fori_loop(1, inner, send, 0)

    names["res"].wait()
    for p in others:
        row_copy(me, r_line.at[zo], p * inner + xi).start()
    to_plane(zo)

    pairs = [(eg_hbm.at[0], eg.at[core]), (eu_hbm.at[0], eu.at[core]), (ed_hbm.at[0], own_down)]
    w_copies = [
        pltpu.make_async_remote_copy(
            src_ref=a,
            dst_ref=b,
            send_sem=w_send.at[k],
            recv_sem=w_recv.at[k],
            device_id={"tp": other},
            device_id_type=MESH,
        )
        for k, (a, b) in enumerate(pairs)
    ]
    for c in w_copies:
        c.start()

    top = jnp.maximum(jnp.max(scores, -1, keepdims=True), own)
    probs = jnp.exp(scores - top)
    own_p = jnp.exp(own - top)
    total = row_sum(probs) + own_p
    weights = probs / total
    own_w = (own_p / total).astype(BF16).astype(F32)
    for s in range(seqs):
        at = slice(s * heads, (s + 1) * heads)
        lat[at, :] = dot(weights[at].astype(BF16), cache[s]) + own_w[at] * ln_all[s : s + 1]

    names["vu"].wait()
    wide = dot_nt(lat[...].astype(BF16), vu[...])
    hv = wide.shape[1]
    vdim = hv // heads
    wide = wide.reshape(seqs, heads, hv)
    h_row = lax.broadcasted_iota(jnp.int32, wide.shape, 1)
    h_lane = lax.broadcasted_iota(jnp.int32, wide.shape, 2)
    own_head = (h_lane >= h_row * vdim) & (h_lane < (h_row + 1) * vdim)
    heads_all[me] = jnp.sum(jnp.where(own_head, wide, 0.0), 1).astype(BF16)

    def head_copy(target):
        return pltpu.make_async_remote_copy(
            src_ref=heads_all.at[me],
            dst_ref=heads_all.at[me],
            send_sem=h_send,
            recv_sem=h_recv.at[zo],
            device_id={"ep": target},
            device_id_type=MESH,
        )

    for p in others:

        def send_line(i, carry):
            head_copy(p * inner + lax.rem(xi + i, inner)).start()
            return carry

        lax.fori_loop(0, inner, send_line, 0)

    def send_mate(d, carry):
        head_copy(mate(d)).start()
        return carry

    lax.fori_loop(1, inner, send_mate, 0)

    for p in reversed(others):
        row_copy(p * inner + xi, r_line.at[p], me).wait_recv()
        to_plane(p)
    order = [zo] + others[::-1]

    def block_wait(ref, send_sem, recv_sem):
        return pltpu.make_async_remote_copy(
            src_ref=ref,
            dst_ref=ref,
            send_sem=send_sem,
            recv_sem=recv_sem,
            device_id={"ep": me},
            device_id_type=MESH,
        )

    for name in ("op", "ag", "mg"):
        names[name].wait()
    tile = 512 if width % 512 == 0 else width
    tiles = width // tile
    slices = [slice(t * tile, (t + 1) * tile) for t in range(tiles)]

    def vector(ref, cols):
        return ref[cols].astype(F32).reshape(1, tile)

    def flat(ref, planes, cols):
        parts = []
        for p in planes:
            block = ref[pl.ds(p * inner, inner), :, cols].astype(F32)
            parts.append(block.reshape(plane_rows, block.shape[-1]))
        return parts[0] if len(parts) == 1 else jnp.concatenate(parts, 0)

    rows = group * plane_rows
    for c in range(outer // group):
        planes = order[c * group : (c + 1) * group]
        for k, p in enumerate(planes):
            own_plane = c == 0 and k == 0
            count = inner - 1 if own_plane else inner
            block_wait(heads_all.at[pl.ds(0, count)], h_send, h_recv.at[p]).wait_recv()
            block_wait(rows_all.at[pl.ds(0, inner - 1)], r_send, r_plane.at[p]).wait_recv()
        x = flat(heads_all, planes, slice(0, hv)).astype(BF16)
        total = jnp.zeros((rows, 1), F32)
        for cols in slices:
            attn = dot(x, op[:, cols]).astype(BF16).astype(F32)
            value = ALPHA * flat(rows_all, planes, cols) + attn
            wide_rows[:, cols] = value
            total = total + row_sum(value)
        center = total / width
        spread = jnp.zeros((rows, 1), F32)
        for cols in slices:
            spread = spread + row_sum(jnp.square(wide_rows[:, cols] - center))
        inv = lax.rsqrt(spread / width + EPS)
        gate = jnp.zeros((rows, 1), F32)
        for cols in slices:
            value = (wide_rows[:, cols] - center) * inv * vector(attn_gain, cols)
            value = value.astype(BF16)
            for k, p in enumerate(planes):
                at = pl.ds(pl.multiple_of(p * plane_rows, plane_rows), plane_rows)
                mixed[at, cols] = value[k * plane_rows : (k + 1) * plane_rows]
            gate = gate + row_sum(value.astype(F32) * vector(mix_gate, cols))
        blend = 1.0 / (1.0 + jnp.exp(-gate))
        tail = flat(rows_all, planes, slice(width, width + extra))
        c_lane = lax.broadcasted_iota(jnp.int32, (rows, extra), 1)
        weight = row_sum(jnp.where((c_lane == me) | (c_lane == me + n), tail, 0.0))
        s_lane = lax.broadcasted_iota(jnp.int32, (rows, 128), 1)
        both = jnp.where(s_lane == 0, weight, blend)
        for k, p in enumerate(planes):
            at = pl.ds(pl.multiple_of(p * plane_rows, plane_rows), plane_rows)
            scale[at, :] = both[k * plane_rows : (k + 1) * plane_rows]

    for name in ("eg", "eu", "ed", "dg", "du", "dd", "og"):
        names[name].wait()
    for c in w_copies:
        c.wait_recv()

    chunk = min(n * seqs, 128)

    def hidden(b, carry):
        at = pl.ds(pl.multiple_of(b * chunk, chunk), chunk)
        x = mixed[at, :]
        both = scale[at, :]
        weight, blend = both[:, 0:1], both[:, 1:2]
        for j in range(2):
            value = silu(dot(x, eg[j])) * dot(x, eu[j]) * weight
            hid[at, j * half_fe : (j + 1) * half_fe] = value.astype(BF16)
        value = silu(dot(x, dg[...])) * dot(x, du[...]) * blend
        hid[at, 2 * half_fe :] = value.astype(BF16)
        return carry

    lax.fori_loop(0, n * seqs // chunk, hidden, 0)

    def plane_copy(p, d, target):
        return pltpu.make_async_remote_copy(
            src_ref=sbuf.at[p, lax.rem(xi + d, inner)],
            dst_ref=rbuf.at[p, d],
            send_sem=s_send,
            recv_sem=s_plane.at[p],
            device_id={"ep": target},
            device_id_type=MESH,
        )

    for p in others + [zo]:
        at = pl.ds(pl.multiple_of(p * plane_rows, plane_rows), plane_rows)
        part = dot(hid[at, :], down[...])
        sbuf[p] = part.reshape(inner, seqs, width).astype(BF16)

        def send(d, carry):
            plane_copy(p, d, mate(d)).start()
            return carry

        lax.fori_loop(1, inner, send, 0)

    def plane_sum(p, start):
        block_wait(rbuf.at[p, pl.ds(1, inner - 1)], s_send, s_plane.at[p]).wait_recv()

        def one(d, total):
            return total + rbuf[p, d].astype(F32)

        return lax.fori_loop(1, inner, one, start, unroll=inner <= 4)

    for p in others:
        zbuf[p] = plane_sum(p, sbuf[p, xi].astype(F32)).astype(BF16)
        pltpu.make_async_remote_copy(
            src_ref=zbuf.at[p],
            dst_ref=zrecv.at[zo],
            send_sem=s_send,
            recv_sem=s_line,
            device_id={"ep": p * inner + xi},
            device_id_type=MESH,
        ).start()

    pair = mixed[pl.ds(pl.multiple_of(lax.div(me, 2) * 2 * seqs, 2 * seqs), 2 * seqs), :]
    pair = pair.astype(F32).reshape(2, seqs, width)
    odd = lax.rem(me, 2).astype(F32)
    start = ALPHA * (pair[0] + odd * (pair[1] - pair[0]))
    total = plane_sum(zo, start + sbuf[zo, xi].astype(F32))
    if outer > 1:
        block_wait(zrecv.at[pl.ds(0, outer - 1)], s_send, s_line).wait_recv()
    for p in others:
        total = total + zrecv[p].astype(F32)
    center = row_sum(total) / width
    shifted = total - center
    spread = row_sum(jnp.square(shifted)) / width
    gain = out_gain[...].astype(F32).reshape(1, width)
    out[...] = (shifted * lax.rsqrt(spread + EPS) * gain).astype(BF16)

    block_wait(rows_all.at[pl.ds(0, n - 1)], r_send, r_line.at[0]).wait_send()
    block_wait(heads_all.at[pl.ds(0, n - 1)], h_send, h_recv.at[0]).wait_send()
    for p in others:
        block_wait(rbuf.at[p], s_send, s_line).wait_send()
    block_wait(rbuf.at[zo, pl.ds(0, inner - 1)], s_send, s_line).wait_send()
    for c in w_copies:
        c.wait_send()


def on_device(
    n,
    residual,
    query_latent,
    query_rotary,
    latent_new,
    rotary_new,
    latent_cache,
    rotary_cache,
    lengths,
    value_up,
    out_proj,
    attn_gain,
    mix_gate,
    dense_w_gate,
    dense_w_up,
    dense_w_down,
    expert_ids,
    expert_scores,
    expert_gate,
    expert_up,
    expert_down,
    out_gain,
):
    seqs, width = residual.shape
    heads = query_latent.shape[1]
    vu = value_up.transpose(1, 2, 0).reshape(-1, value_up.shape[0])
    rotary_turned = rotary_cache.transpose(0, 2, 1)
    extra = -(-2 * n // 128) * 128
    inner = inner_size(n)
    outer = n // inner
    group = max(1, min(outer, 128 // (inner * seqs)))
    while outer % group:
        group -= 1
    hbm = pl.BlockSpec(memory_space=pl.ANY)
    smem = pl.BlockSpec(memory_space=pltpu.SMEM)
    dma = pltpu.SemaphoreType.DMA
    block = (outer, inner, seqs, width)
    half_fe = expert_gate.shape[-1]
    fd = dense_w_gate.shape[-1]
    return pl.pallas_call(
        functools.partial(kernel, n, group),
        out_shape=pltpu.VMEM((seqs, width), BF16),
        in_specs=[smem] + [hbm] * 20,
        out_specs=pl.BlockSpec(memory_space=VMEM),
        scratch_shapes=[
            VMEM(query_rotary.shape, BF16),
            VMEM(rotary_new.shape, BF16),
            VMEM(query_latent.shape, BF16),
            VMEM(latent_new.shape, BF16),
            VMEM(rotary_turned.shape, BF16),
            VMEM(latent_cache.shape, BF16),
            VMEM(expert_ids.shape, jnp.int32),
            VMEM(expert_scores.shape, F32),
            VMEM(vu.shape, BF16),
            VMEM(out_proj.shape, BF16),
            VMEM(attn_gain.shape, BF16),
            VMEM(mix_gate.shape, BF16),
            VMEM((2,) + expert_gate.shape[1:], BF16),
            VMEM((2,) + expert_up.shape[1:], BF16),
            VMEM((2 * half_fe + fd, width), BF16),
            VMEM(dense_w_gate.shape, BF16),
            VMEM(dense_w_up.shape, BF16),
            VMEM(out_gain.shape, BF16),
            VMEM((seqs * heads, latent_cache.shape[-1]), F32),
            VMEM((n, seqs, width + extra), BF16),
            VMEM((n, seqs, vu.shape[0]), BF16),
            VMEM((group * inner * seqs, width), F32),
            VMEM((n * seqs, width), BF16),
            VMEM((n * seqs, 128), F32),
            VMEM((n * seqs, 2 * half_fe + fd), BF16),
            VMEM(block, BF16),
            VMEM(block, BF16),
            VMEM((outer, seqs, width), BF16),
            VMEM((outer, seqs, width), BF16),
            dma((19,)),
            dma((seqs,)),
            dma((3,)),
            dma((3,)),
            dma,
            dma((outer,)),
            dma((outer,)),
            dma,
            dma((outer,)),
            dma,
            dma((outer,)),
            dma,
        ],
        compiler_params=pltpu.CompilerParams(
            collective_id=0, has_side_effects=True, vmem_limit_bytes=60 * 1024 * 1024
        ),
    )(
        lengths,
        query_rotary,
        rotary_new,
        query_latent,
        latent_new,
        rotary_turned,
        latent_cache,
        residual,
        expert_ids,
        expert_scores,
        vu,
        out_proj,
        attn_gain,
        mix_gate,
        expert_gate,
        expert_up,
        expert_down,
        dense_w_gate,
        dense_w_up,
        dense_w_down,
        out_gain,
    )


def solution(mesh):
    rows = P(("ep", "tp"), None)
    rows3 = P(("ep", "tp"), None, None)
    return jax.shard_map(
        functools.partial(on_device, mesh.shape["ep"]),
        mesh=mesh,
        in_specs=(
            rows,
            rows3,
            rows3,
            rows,
            rows,
            rows3,
            rows3,
            P(("ep", "tp")),
            P(),
            P(),
            P(),
            P(),
            P(None, "ep"),
            P(None, "ep"),
            P("ep", None),
            rows,
            rows,
            P("ep", None, "tp"),
            P("ep", None, "tp"),
            P("ep", "tp", None),
            P(),
        ),
        out_specs=rows,
        check_vma=False,
    )
```

time: 37.9 us -> 31.2 us (0.82)
  Pallas kernels: 36.3 us -> 30.4 us
  local copies, waits for them, and re-layouts: 1.38 us -> 0.62 us
    pallas_call x1, Pallas kernels: 36.3 us -> 30.4 us  [on_device(): pl.pallas_call(functools.partial(kernel, n, group), out_shape=pltpu.VMEM(...]
    unnamed x1, local copies, waits for them, and re-layouts: 1.38 us -> 0.62 us
where the time goes in v1:
time: 31.2 us; the launch traced here: 31 us
  Pallas kernels  30.4 us (97%)
  local copies, waits for them, and re-layouts  0.62 us (2%)
    pallas_call x1, Pallas kernels, on_device(): pl.pallas_call(functools.partial(kernel, n, group), out_shape=pltpu.VMEM(...  30.4 us

profile of v1, /device:TPU:0, one launch (start us, length us, event | category | flops | bytes accessed | tf_op | source)
XLA Modules:
  0.0 31.0 jit_solution(8215135580610994230)
XLA Ops:
  0.0 30.4 %shard_map.199 = bf16[8,2048]{1,0:T(8,128)(2,1)S(1)} custom-call(s32[8]{0:T(128)} %lengths.1, bf16[8,8,32]{2,1,0:T(8,128)(2,1)} %qr_hbm.1, bf16[8,32]{1,0:T(8,128)(2,1)} %rn_hbm.1, bf16[8,8,512]{2,1,0:T(8,128)(2,1)} %ql_hbm.1, bf16[8,512]{1,0:T(8,128)(2,1)} %ln_hbm.1, bf16[8,32,256]{2,1,0:T(8,128)(2,1)} %bitcast.5, bf16[8,256,512]{2,1,0:T(8,128)(2,1)} %cache_hbm.1, ...), custom_call_target="tpu_custom_call" | custom-call | tf_op jit(solution)/shard_map/pallas_call | solution.py:514
  30.4 0.6 %copy.23 = bf16[8,2048]{1,0:T(8,128)(2,1)} copy(bf16[8,2048]{1,0:T(8,128)(2,1)S(1)} %shard_map.199) | data formatting | bytes 65536

commit v2 on v1

--- a/solution.py
+++ b/solution.py
@@ -43,8 +43,8 @@
 
 def kernel(
     n,
-    group,
-    lengths,
+    groups,
+    len_hbm,
     qr_hbm,
     rn_hbm,
     ql_hbm,
@@ -66,6 +66,7 @@
     dd_hbm,
     og_hbm,
     out,
+    lengths,
     query_rotary,
     rotary_new,
     query_latent,
@@ -89,7 +90,7 @@
     heads_all,
     wide_rows,
     mixed,
-    scale,
+    own_mixed,
     hid,
     sbuf,
     rbuf,
@@ -107,6 +108,7 @@
     s_send,
     s_plane,
     s_line,
+    ready,
 ):
     me = lax.axis_index("ep")
     core = lax.axis_index("tp")
@@ -125,11 +127,14 @@
     xi = lax.rem(me, inner)
     upper = lax.div(2 * zo, outer)
 
+    def descend(k):
+        p = outer - 1 - k
+        return p - jnp.where(p <= zo, 1, 0)
+
     def far(k):
-        down_order = outer - 1 - k
-        down_order = down_order - jnp.where(down_order <= zo, 1, 0)
-        up_order = k + jnp.where(zo <= k, 1, 0)
-        return down_order + upper * (up_order - down_order)
+        first = descend(k)
+        lower = first + lax.min(zo, 1) * ((descend(k - 1) if k else 0) - first)
+        return lower + upper * (k + jnp.where(zo <= k, 1, 0) - lower)
 
     others = [far(k) for k in range(outer - 1)]
 
@@ -138,12 +143,16 @@
 
     barrier = pltpu.get_barrier_semaphore()
 
-    def greet(d, carry):
-        peer = lax.rem(me + d, n)
-        pl.semaphore_signal(barrier, inc=1, device_id={"ep": peer}, device_id_type=MESH)
+    def greet(sem, peer):
+        pl.semaphore_signal(sem, inc=1, device_id={"ep": peer}, device_id_type=MESH)
+
+    def greet_mate(d, carry):
+        greet(barrier, mate(d))
         return carry
 
-    lax.fori_loop(1, n, greet, 0)
+    for p in others:
+        greet(barrier, p * inner + xi)
+    lax.fori_loop(1, inner, greet_mate, 0)
     pl.semaphore_signal(barrier, inc=1, device_id={"tp": other}, device_id_type=MESH)
 
     own_down = down.at[pl.ds(pl.multiple_of(core * half_fe, half_fe), half_fe)]
@@ -154,32 +163,23 @@
         c.start()
         names[name] = c
 
+    load("len", len_hbm, lengths)
     load("qr", qr_hbm, query_rotary)
     load("rn", rn_hbm, rotary_new)
     load("ql", ql_hbm, query_latent)
     load("ln", ln_hbm, latent_new)
     load("rc", rc_hbm, rotary_cache)
+    load("res", res_hbm, rows_all.at[me, :, pl.ds(0, width)])
+    load("ids", ids_hbm, ids)
+    load("rs", rs_hbm, route_scores)
     cache_copies = [
         pltpu.make_async_copy(cache_hbm.at[s], cache.at[s], cache_sem.at[s]) for s in range(seqs)
     ]
     for c in cache_copies:
         c.start()
-    load("res", res_hbm, rows_all.at[me, :, pl.ds(0, width)])
-    load("ids", ids_hbm, ids)
-    load("rs", rs_hbm, route_scores)
-    load("vu", vu_hbm, vu)
-    load("op", op_hbm, op)
-    load("ag", ag_hbm, attn_gain)
-    load("mg", mg_hbm, mix_gate)
-    load("eg", eg_hbm.at[0], eg.at[core])
-    load("eu", eu_hbm.at[0], eu.at[core])
-    load("ed", ed_hbm.at[0], own_down)
-    load("dg", dg_hbm, dg)
-    load("du", du_hbm, du)
-    load("dd", dd_hbm, down.at[pl.ds(2 * half_fe, fd)])
-    load("og", og_hbm, out_gain)
 
     half = rope // 2
+    names["len"].wait()
     lane = lax.broadcasted_iota(jnp.int32, (seqs, rope), 1)
     row = lax.broadcasted_iota(jnp.int32, (seqs, rope), 0)
     pos = jnp.zeros((seqs, rope), F32)
@@ -203,21 +203,6 @@
     score_scale = (NOPE + rope) ** (-0.5)
     t_idx = lax.broadcasted_iota(jnp.int32, (heads, cache_len), 1)
 
-    score_rows, own_rows_all = [], []
-    for s in range(seqs):
-        q_turn = (q_rot[s] * cosine[s : s + 1] + q_swap[s] * sine[s : s + 1]).astype(BF16)
-        ql = query_latent[s]
-        own_rows_all.append(
-            row_sum(ql.astype(F32) * ln_all[s : s + 1])
-            + row_sum(q_turn.astype(F32) * k_turn[s : s + 1])
-        )
-        rot_part = dot(q_turn, rotary_cache[s])
-        cache_copies[s].wait()
-        part = dot_nt(ql, cache[s]) + rot_part
-        score_rows.append(jnp.where(t_idx < lengths[s], part, -jnp.inf))
-    own = jnp.concatenate(own_rows_all, 0) * score_scale
-    scores = jnp.concatenate(score_rows, 0) * score_scale
-
     names["ids"].wait()
     names["rs"].wait()
     sc = route_scores[...]
@@ -232,8 +217,6 @@
     coef = jnp.where(low, coef - high.astype(F32), high.astype(F32)).astype(BF16)
     rows_all[me, :, width:] = coef
 
-    pl.semaphore_wait(barrier, n)
-
     def row_copy(block, sem, target):
         return pltpu.make_async_remote_copy(
             src_ref=rows_all.at[block],
@@ -252,11 +235,6 @@
             return carry
 
         lax.fori_loop(1, inner, send, 0)
-
-    names["res"].wait()
-    for p in others:
-        row_copy(me, r_line.at[zo], p * inner + xi).start()
-    to_plane(zo)
 
     pairs = [(eg_hbm.at[0], eg.at[core]), (eu_hbm.at[0], eu.at[core]), (ed_hbm.at[0], own_down)]
     w_copies = [
@@ -270,8 +248,50 @@
         )
         for k, (a, b) in enumerate(pairs)
     ]
-    for c in w_copies:
-        c.start()
+    def announce():
+        pl.semaphore_wait(barrier, outer + inner - 1)
+        for p in others:
+            greet(ready, p * inner + xi)
+        for p in others:
+            row_copy(me, r_line.at[zo], p * inner + xi).start()
+        to_plane(zo)
+        for c in w_copies:
+            c.start()
+
+    names["res"].wait()
+    @pl.when(upper == 1)
+    def _():
+        announce()
+
+    score_rows, own_rows_all = [], []
+    for s in range(seqs):
+        q_turn = (q_rot[s] * cosine[s : s + 1] + q_swap[s] * sine[s : s + 1]).astype(BF16)
+        ql = query_latent[s]
+        own_rows_all.append(
+            row_sum(ql.astype(F32) * ln_all[s : s + 1])
+            + row_sum(q_turn.astype(F32) * k_turn[s : s + 1])
+        )
+        rot_part = dot(q_turn, rotary_cache[s])
+        cache_copies[s].wait()
+        part = dot_nt(ql, cache[s]) + rot_part
+        score_rows.append(jnp.where(t_idx < lengths[s], part, -jnp.inf))
+    load("vu", vu_hbm, vu)
+    load("op", op_hbm, op)
+    load("ag", ag_hbm, attn_gain)
+    load("mg", mg_hbm, mix_gate)
+    load("eg", eg_hbm.at[0], eg.at[core])
+    load("eu", eu_hbm.at[0], eu.at[core])
+    load("ed", ed_hbm.at[0], own_down)
+    load("dg", dg_hbm, dg)
+    load("du", du_hbm, du)
+    load("dd", dd_hbm, down.at[pl.ds(2 * half_fe, fd)])
+    load("og", og_hbm, out_gain)
+    own = jnp.concatenate(own_rows_all, 0) * score_scale
+    scores = jnp.concatenate(score_rows, 0) * score_scale
+
+    @pl.when(upper == 0)
+    def _():
+        announce()
 
     top = jnp.maximum(jnp.max(scores, -1, keepdims=True), own)
     probs = jnp.exp(scores - top)
@@ -293,6 +313,9 @@
     own_head = (h_lane >= h_row * vdim) & (h_lane < (h_row + 1) * vdim)
     heads_all[me] = jnp.sum(jnp.where(own_head, wide, 0.0), 1).astype(BF16)
 
+    if outer > 1:
+        pl.semaphore_wait(ready, outer - 1)
+
     def head_copy(target):
         return pltpu.make_async_remote_copy(
             src_ref=heads_all.at[me],
@@ -317,10 +340,10 @@
 
     lax.fori_loop(1, inner, send_mate, 0)
 
-    for p in reversed(others):
+    for p in others:
         row_copy(p * inner + xi, r_line.at[p], me).wait_recv()
         to_plane(p)
-    order = [zo] + others[::-1]
+    order = others + [zo]
 
     def block_wait(ref, send_sem, recv_sem):
         return pltpu.make_async_remote_copy(
@@ -348,65 +371,6 @@
             parts.append(block.reshape(plane_rows, block.shape[-1]))
         return parts[0] if len(parts) == 1 else jnp.concatenate(parts, 0)
 
-    rows = group * plane_rows
-    for c in range(outer // group):
-        planes = order[c * group : (c + 1) * group]
-        for k, p in enumerate(planes):
-            own_plane = c == 0 and k == 0
-            count = inner - 1 if own_plane else inner
-            block_wait(heads_all.at[pl.ds(0, count)], h_send, h_recv.at[p]).wait_recv()
-            block_wait(rows_all.at[pl.ds(0, inner - 1)], r_send, r_plane.at[p]).wait_recv()
-        x = flat(heads_all, planes, slice(0, hv)).astype(BF16)
-        total = jnp.zeros((rows, 1), F32)
-        for cols in slices:
-            attn = dot(x, op[:, cols]).astype(BF16).astype(F32)
-            value = ALPHA * flat(rows_all, planes, cols) + attn
-            wide_rows[:, cols] = value
-            total = total + row_sum(value)
-        center = total / width
-        spread = jnp.zeros((rows, 1), F32)
-        for cols in slices:
-            spread = spread + row_sum(jnp.square(wide_rows[:, cols] - center))
-        inv = lax.rsqrt(spread / width + EPS)
-        gate = jnp.zeros((rows, 1), F32)
-        for cols in slices:
-            value = (wide_rows[:, cols] - center) * inv * vector(attn_gain, cols)
-            value = value.astype(BF16)
-            for k, p in enumerate(planes):
-                at = pl.ds(pl.multiple_of(p * plane_rows, plane_rows), plane_rows)
-                mixed[at, cols] = value[k * plane_rows : (k + 1) * plane_rows]
-            gate = gate + row_sum(value.astype(F32) * vector(mix_gate, cols))
-        blend = 1.0 / (1.0 + jnp.exp(-gate))
-        tail = flat(rows_all, planes, slice(width, width + extra))
-        c_lane = lax.broadcasted_iota(jnp.int32, (rows, extra), 1)
-        weight = row_sum(jnp.where((c_lane == me) | (c_lane == me + n), tail, 0.0))
-        s_lane = lax.broadcasted_iota(jnp.int32, (rows, 128), 1)
-        both = jnp.where(s_lane == 0, weight, blend)
-        for k, p in enumerate(planes):
-            at = pl.ds(pl.multiple_of(p * plane_rows, plane_rows), plane_rows)
-            scale[at, :] = both[k * plane_rows : (k + 1) * plane_rows]
-
-    for name in ("eg", "eu", "ed", "dg", "du", "dd", "og"):
-        names[name].wait()
-    for c in w_copies:
-        c.wait_recv()
-
-    chunk = min(n * seqs, 128)
-
-    def hidden(b, carry):
-        at = pl.ds(pl.multiple_of(b * chunk, chunk), chunk)
-        x = mixed[at, :]
-        both = scale[at, :]
-        weight, blend = both[:, 0:1], both[:, 1:2]
-        for j in range(2):
-            value = silu(dot(x, eg[j])) * dot(x, eu[j]) * weight
-            hid[at, j * half_fe : (j + 1) * half_fe] = value.astype(BF16)
-        value = silu(dot(x, dg[...])) * dot(x, du[...]) * blend
-        hid[at, 2 * half_fe :] = value.astype(BF16)
-        return carry
-
-    lax.fori_loop(0, n * seqs // chunk, hidden, 0)
-
     def plane_copy(p, d, target):
         return pltpu.make_async_remote_copy(
             src_ref=sbuf.at[p, lax.rem(xi + d, inner)],
@@ -417,16 +381,65 @@
             device_id_type=MESH,
         )
 
-    for p in others + [zo]:
-        at = pl.ds(pl.multiple_of(p * plane_rows, plane_rows), plane_rows)
-        part = dot(hid[at, :], down[...])
-        sbuf[p] = part.reshape(inner, seqs, width).astype(BF16)
-
-        def send(d, carry):
-            plane_copy(p, d, mate(d)).start()
-            return carry
-
-        lax.fori_loop(1, inner, send, 0)
+    chunks = len(groups)
+    for c in range(chunks):
+        group = groups[c]
+        rows = group * plane_rows
+        planes = order[sum(groups[:c]) : sum(groups[: c + 1])]
+        for k, p in enumerate(planes):
+            own_plane = c == chunks - 1 and k == group - 1
+            count = inner - 1 if own_plane else inner
+            block_wait(heads_all.at[pl.ds(0, count)], h_send, h_recv.at[p]).wait_recv()
+            block_wait(rows_all.at[pl.ds(0, inner - 1)], r_send, r_plane.at[p]).wait_recv()
+        x = flat(heads_all, planes, slice(0, hv)).astype(BF16)
+        total = jnp.zeros((rows, 1), F32)
+        for cols in slices:
+            attn = dot(x, op[:, cols]).astype(BF16).astype(F32)
+            value = ALPHA * flat(rows_all, planes, cols) + attn
+            wide_rows[:rows, cols] = value
+            total = total + row_sum(value)
+        center = total / width
+        spread = jnp.zeros((rows, 1), F32)
+        for cols in slices:
+            spread = spread + row_sum(jnp.square(wide_rows[:rows, cols] - center))
+        inv = lax.rsqrt(spread / width + EPS)
+        gate = jnp.zeros((rows, 1), F32)
+        for cols in slices:
+            value = (wide_rows[:rows, cols] - center) * inv * vector(attn_gain, cols)
+            value = value.astype(BF16)
+            mixed[:rows, cols] = value
+            if c == chunks - 1:
+                own_mixed[:, cols] = value[rows - plane_rows :]
+            gate = gate + row_sum(value.astype(F32) * vector(mix_gate, cols))
+        blend = 1.0 / (1.0 + jnp.exp(-gate))
+        tail = flat(rows_all, planes, slice(width, width + extra))
+        c_lane = lax.broadcasted_iota(jnp.int32, (rows, extra), 1)
+        weight = row_sum(jnp.where((c_lane == me) | (c_lane == me + n), tail, 0.0))
+
+        if c == 0:
+            for name in ("eg", "eu", "ed", "dg", "du", "dd", "og"):
+                names[name].wait()
+            for w in w_copies:
+                w.wait_recv()
+        x = mixed[:rows, :]
+        for j in range(2):
+            value = silu(dot(x, eg[j])) * dot(x, eu[j]) * weight
+            hid[:rows, j * half_fe : (j + 1) * half_fe] = value.astype(BF16)
+        value = silu(dot(x, dg[...])) * dot(x, du[...]) * blend
+        hid[:rows, 2 * half_fe :] = value.astype(BF16)
+
+        for cols in slices:
+            part = dot(hid[:rows, :], down[:, cols])
+            for k, p in enumerate(planes):
+                block = part[k * plane_rows : (k + 1) * plane_rows].reshape(inner, seqs, tile)
+                sbuf[p, :, :, cols] = block.astype(BF16)
+        for p in planes:
+
+            def send(d, carry):
+                plane_copy(p, d, mate(d)).start()
+                return carry
+
+            lax.fori_loop(1, inner, send, 0)
 
     def plane_sum(p, start):
         block_wait(rbuf.at[p, pl.ds(1, inner - 1)], s_send, s_plane.at[p]).wait_recv()
@@ -447,9 +460,10 @@
             device_id_type=MESH,
         ).start()
 
-    pair = mixed[pl.ds(pl.multiple_of(lax.div(me, 2) * 2 * seqs, 2 * seqs), 2 * seqs), :]
+    at = pl.ds(pl.multiple_of(lax.div(xi, 2) * 2 * seqs, 2 * seqs), 2 * seqs)
+    pair = own_mixed[at, :]
     pair = pair.astype(F32).reshape(2, seqs, width)
-    odd = lax.rem(me, 2).astype(F32)
+    odd = lax.rem(xi, 2).astype(F32)
     start = ALPHA * (pair[0] + odd * (pair[1] - pair[0]))
     total = plane_sum(zo, start + sbuf[zo, xi].astype(F32))
     if outer > 1:
@@ -502,21 +516,23 @@
     extra = -(-2 * n // 128) * 128
     inner = inner_size(n)
     outer = n // inner
-    group = max(1, min(outer, 128 // (inner * seqs)))
-    while outer % group:
-        group -= 1
+    most = max(1, 128 // (inner * seqs))
+    groups = [1]
+    while sum(groups) < outer:
+        groups.append(min(most, outer - sum(groups)))
+    top = max(groups) * inner * seqs
     hbm = pl.BlockSpec(memory_space=pl.ANY)
-    smem = pl.BlockSpec(memory_space=pltpu.SMEM)
     dma = pltpu.SemaphoreType.DMA
     block = (outer, inner, seqs, width)
     half_fe = expert_gate.shape[-1]
     fd = dense_w_gate.shape[-1]
     return pl.pallas_call(
-        functools.partial(kernel, n, group),
+        functools.partial(kernel, n, tuple(groups)),
         out_shape=pltpu.VMEM((seqs, width), BF16),
-        in_specs=[smem] + [hbm] * 20,
+        in_specs=[hbm] * 21,
         out_specs=pl.BlockSpec(memory_space=VMEM),
         scratch_shapes=[
+            pltpu.SMEM(lengths.shape, jnp.int32),
             VMEM(query_rotary.shape, BF16),
             VMEM(rotary_new.shape, BF16),
             VMEM(query_latent.shape, BF16),
@@ -538,15 +554,15 @@
             VMEM((seqs * heads, latent_cache.shape[-1]), F32),
             VMEM((n, seqs, width + extra), BF16),
             VMEM((n, seqs, vu.shape[0]), BF16),
-            VMEM((group * inner * seqs, width), F32),
-            VMEM((n * seqs, width), BF16),
-            VMEM((n * seqs, 128), F32),
-            VMEM((n * seqs, 2 * half_fe + fd), BF16),
+            VMEM((top, width), F32),
+            VMEM((top, width), BF16),
+            VMEM((inner * seqs, width), BF16),
+            VMEM((top, 2 * half_fe + fd), BF16),
             VMEM(block, BF16),
             VMEM(block, BF16),
             VMEM((outer, seqs, width), BF16),
             VMEM((outer, seqs, width), BF16),
-            dma((19,)),
+            dma((20,)),
             dma((seqs,)),
             dma((3,)),
             dma((3,)),
@@ -558,6 +574,7 @@
             dma,
             dma((outer,)),
             dma,
+            pltpu.SemaphoreType.REGULAR,
         ],
         compiler_params=pltpu.CompilerParams(
             collective_id=0, has_side_effects=True, vmem_limit_bytes=60 * 1024 * 1024

time: 31.2 us -> 26.5 us (0.85); the launches traced: 31 us -> 26 us
  Pallas kernels: 30.4 us -> 25.4 us
    pallas_call x1, Pallas kernels: 30.4 us -> 25.4 us  [on_device(): pl.pallas_call(functools.partial(kernel, n, tuple(groups)), out_shape=plt...]
where the time goes in v2:
time: 26.5 us; the launch traced here: 26 us
  Pallas kernels  25.4 us (96%)
  local copies, waits for them, and re-layouts  0.62 us (2%)
    pallas_call x1, Pallas kernels, on_device(): pl.pallas_call(functools.partial(kernel, n, tuple(groups)), out_shape=plt...  25.4 us
    unnamed x1, local copies, waits for them, and re-layouts  0.62 us

profile of v2, /device:TPU:0, one launch (start us, length us, event | category | flops | bytes accessed | tf_op | source)
XLA Modules:
  0.0 26.0 jit_solution(13978169812805987122)
XLA Ops:
  0.0 25.4 %shard_map.199 = bf16[8,2048]{1,0:T(8,128)(2,1)S(1)} custom-call(s32[8]{0:T(128)} %len_hbm.1, bf16[8,8,32]{2,1,0:T(8,128)(2,1)} %qr_hbm.1, bf16[8,32]{1,0:T(8,128)(2,1)} %rn_hbm.1, bf16[8,8,512]{2,1,0:T(8,128)(2,1)} %ql_hbm.1, bf16[8,512]{1,0:T(8,128)(2,1)} %ln_hbm.1, bf16[8,32,256]{2,1,0:T(8,128)(2,1)} %bitcast.5, bf16[8,256,512]{2,1,0:T(8,128)(2,1)} %cache_hbm.1, ...), custom_call_target="tpu_custom_call" | custom-call | tf_op jit(solution)/shard_map/pallas_call | solution.py:529
  25.4 0.6 %copy.23 = bf16[8,2048]{1,0:T(8,128)(2,1)} copy(bf16[8,2048]{1,0:T(8,128)(2,1)S(1)} %shard_map.199) | data formatting | bytes 65536

commit v3 on v2

--- a/solution.py
+++ b/solution.py
@@ -109,6 +109,9 @@
     s_plane,
     s_line,
     ready,
+    obuf,
+    yout,
+    o_plane,
 ):
     me = lax.axis_index("ep")
     core = lax.axis_index("tp")
@@ -252,6 +255,7 @@
         pl.semaphore_wait(barrier, outer + inner - 1)
         for p in others:
             greet(ready, p * inner + xi)
+
         for p in others:
             row_copy(me, r_line.at[zo], p * inner + xi).start()
         to_plane(zo)
@@ -272,7 +276,9 @@
             + row_sum(q_turn.astype(F32) * k_turn[s : s + 1])
         )
         rot_part = dot(q_turn, rotary_cache[s])
-        cache_copies[s].wait()
+        if s % 8 == 0:
+            for c in cache_copies[s : s + 8]:
+                c.wait()
         part = dot_nt(ql, cache[s]) + rot_part
         score_rows.append(jnp.where(t_idx < lengths[s], part, -jnp.inf))
     load("vu", vu_hbm, vu)
@@ -340,9 +346,6 @@
 
     lax.fori_loop(1, inner, send_mate, 0)
 
-    for p in others:
-        row_copy(p * inner + xi, r_line.at[p], me).wait_recv()
-        to_plane(p)
     order = others + [zo]
 
     def block_wait(ref, send_sem, recv_sem):
@@ -355,6 +358,10 @@
             device_id_type=MESH,
         )
 
+    for p in others:
+        row_copy(p * inner + xi, r_line.at[p], me).wait_recv()
+        to_plane(p)
+
     for name in ("op", "ag", "mg"):
         names[name].wait()
     tile = 512 if width % 512 == 0 else width
@@ -371,15 +378,22 @@
             parts.append(block.reshape(plane_rows, block.shape[-1]))
         return parts[0] if len(parts) == 1 else jnp.concatenate(parts, 0)
 
-    def plane_copy(p, d, target):
+    def plane_copy(p, d, dst, sem, c):
         return pltpu.make_async_remote_copy(
             src_ref=sbuf.at[p, lax.rem(xi + d, inner)],
-            dst_ref=rbuf.at[p, d],
+            dst_ref=dst.at[p, d],
             send_sem=s_send,
-            recv_sem=s_plane.at[p],
-            device_id={"ep": target},
+            recv_sem=sem.at[p],
+            device_id={"ep": mate(d), "tp": c},
             device_id_type=MESH,
         )
+
+    def plane_send(p, dst, sem, c, first):
+        def send(d, carry):
+            plane_copy(p, d, dst, sem, c).start()
+            return carry
+
+        lax.fori_loop(first, inner, send, 0)
 
     chunks = len(groups)
     for c in range(chunks):
@@ -433,13 +447,18 @@
             for k, p in enumerate(planes):
                 block = part[k * plane_rows : (k + 1) * plane_rows].reshape(inner, seqs, tile)
                 sbuf[p, :, :, cols] = block.astype(BF16)
-        for p in planes:
-
-            def send(d, carry):
-                plane_copy(p, d, mate(d)).start()
-                return carry
-
-            lax.fori_loop(1, inner, send, 0)
+        for k, p in enumerate(planes):
+            if c == chunks - 1 and k == group - 1:
+                plane_send(p, rbuf, s_plane, core, 1)
+            else:
+
+                @pl.when(core == 1)
+                def _():
+                    plane_send(p, rbuf, s_plane, core, 1)
+
+                @pl.when(core == 0)
+                def _():
+                    plane_send(p, obuf, o_plane, other, 0)
 
     def plane_sum(p, start):
         block_wait(rbuf.at[p, pl.ds(1, inner - 1)], s_send, s_plane.at[p]).wait_recv()
@@ -449,16 +468,30 @@
 
         return lax.fori_loop(1, inner, one, start, unroll=inner <= 4)
 
-    for p in others:
-        zbuf[p] = plane_sum(p, sbuf[p, xi].astype(F32)).astype(BF16)
+    def line_send(src, p, c):
         pltpu.make_async_remote_copy(
-            src_ref=zbuf.at[p],
+            src_ref=src.at[p],
             dst_ref=zrecv.at[zo],
             send_sem=s_send,
             recv_sem=s_line,
-            device_id={"ep": p * inner + xi},
+            device_id={"ep": p * inner + xi, "tp": c},
             device_id_type=MESH,
         ).start()
+
+    @pl.when(core == 1)
+    def _():
+        for p in others:
+            zbuf[p] = plane_sum(p, sbuf[p, xi].astype(F32)).astype(BF16)
+            line_send(zbuf, p, core)
+            block_wait(obuf.at[p], s_send, o_plane.at[p]).wait_recv()
+
+            def one(d, total):
+                return total + obuf[p, d].astype(F32)
+
+            start = obuf[p, 0].astype(F32)
+            total = lax.fori_loop(1, inner, one, start, unroll=inner <= 4)
+            yout[p] = total.astype(BF16)
+            line_send(yout, p, other)
 
     at = pl.ds(pl.multiple_of(lax.div(xi, 2) * 2 * seqs, 2 * seqs), 2 * seqs)
     pair = own_mixed[at, :]
@@ -476,11 +509,24 @@
     gain = out_gain[...].astype(F32).reshape(1, width)
     out[...] = (shifted * lax.rsqrt(spread + EPS) * gain).astype(BF16)
 
-    block_wait(rows_all.at[pl.ds(0, n - 1)], r_send, r_line.at[0]).wait_send()
-    block_wait(heads_all.at[pl.ds(0, n - 1)], h_send, h_recv.at[0]).wait_send()
-    for p in others:
-        block_wait(rbuf.at[p], s_send, s_line).wait_send()
-    block_wait(rbuf.at[zo, pl.ds(0, inner - 1)], s_send, s_line).wait_send()
+    def sent(ref, sem):
+        block_wait(ref, sem, s_line).wait_send()
+
+    sent(heads_all.at[pl.ds(0, n - 1)], h_send)
+    sent(rows_all.at[pl.ds(0, n - 1)], r_send)
+    sent(rbuf.at[zo, pl.ds(0, inner - 1)], s_send)
+
+    @pl.when(core == 1)
+    def _():
+        for p in others:
+            sent(rbuf.at[p, pl.ds(0, inner - 1)], s_send)
+            sent(zrecv.at[pl.ds(0, 2)], s_send)
+
+    @pl.when(core == 0)
+    def _():
+        for p in others:
+            sent(rbuf.at[p], s_send)
+
     for c in w_copies:
         c.wait_send()
 
@@ -575,6 +621,9 @@
             dma((outer,)),
             dma,
             pltpu.SemaphoreType.REGULAR,
+            VMEM(block, BF16),
+            VMEM((outer, seqs, width), BF16),
+            dma((outer,)),
         ],
         compiler_params=pltpu.CompilerParams(
             collective_id=0, has_side_effects=True, vmem_limit_bytes=60 * 1024 * 1024

time: 26.5 us -> 25.4 us (0.958); the launches traced: 26 us -> 25.3 us
  Pallas kernels: 25.4 us -> 24.7 us
    pallas_call x1, Pallas kernels: 25.4 us -> 24.7 us  [on_device(): pl.pallas_call(functools.partial(kernel, n, tuple(groups)), out_shape=plt...]
where the time goes in v3:
time: 25.4 us; the launch traced here: 25.3 us
  Pallas kernels  24.7 us (97%)
  local copies, waits for them, and re-layouts  0.62 us (2%)
    pallas_call x1, Pallas kernels, on_device(): pl.pallas_call(functools.partial(kernel, n, tuple(groups)), out_shape=plt...  24.7 us
    unnamed x1, local copies, waits for them, and re-layouts  0.62 us

profile of v3, /device:TPU:0, one launch (start us, length us, event | category | flops | bytes accessed | tf_op | source)
XLA Modules:
  0.0 25.3 jit_solution(13926347149409886863)
XLA Ops:
  0.0 24.7 %shard_map.199 = bf16[8,2048]{1,0:T(8,128)(2,1)S(1)} custom-call(s32[8]{0:T(128)} %len_hbm.1, bf16[8,8,32]{2,1,0:T(8,128)(2,1)} %qr_hbm.1, bf16[8,32]{1,0:T(8,128)(2,1)} %rn_hbm.1, bf16[8,8,512]{2,1,0:T(8,128)(2,1)} %ql_hbm.1, bf16[8,512]{1,0:T(8,128)(2,1)} %ln_hbm.1, bf16[8,32,256]{2,1,0:T(8,128)(2,1)} %bitcast.5, bf16[8,256,512]{2,1,0:T(8,128)(2,1)} %cache_hbm.1, ...), custom_call_target="tpu_custom_call" | custom-call | tf_op jit(solution)/shard_map/pallas_call | solution.py:575
  24.7 0.6 %copy.23 = bf16[8,2048]{1,0:T(8,128)(2,1)} copy(bf16[8,2048]{1,0:T(8,128)(2,1)S(1)} %shard_map.199) | data formatting | bytes 65536

commit v4 on v3

--- a/solution.py
+++ b/solution.py
@@ -176,7 +176,7 @@
     load("ids", ids_hbm, ids)
     load("rs", rs_hbm, route_scores)
     cache_copies = [
-        pltpu.make_async_copy(cache_hbm.at[s], cache.at[s], cache_sem.at[s]) for s in range(seqs)
+        pltpu.make_async_copy(cache_hbm.at[s], cache.at[s], cache_sem) for s in range(seqs)
     ]
     for c in cache_copies:
         c.start()
@@ -276,9 +276,8 @@
             + row_sum(q_turn.astype(F32) * k_turn[s : s + 1])
         )
         rot_part = dot(q_turn, rotary_cache[s])
-        if s % 8 == 0:
-            for c in cache_copies[s : s + 8]:
-                c.wait()
+        if s == 0:
+            pltpu.make_async_copy(cache_hbm, cache, cache_sem).wait()
         part = dot_nt(ql, cache[s]) + rot_part
         score_rows.append(jnp.where(t_idx < lengths[s], part, -jnp.inf))
     load("vu", vu_hbm, vu)
@@ -286,11 +285,15 @@
     load("ag", ag_hbm, attn_gain)
     load("mg", mg_hbm, mix_gate)
     load("eg", eg_hbm.at[0], eg.at[core])
-    load("eu", eu_hbm.at[0], eu.at[core])
+    pltpu.make_async_copy(eu_hbm.at[0], eu.at[core], in_sem.at[len(names) - 1]).start()
+    names["eg"] = pltpu.make_async_copy(eg, eg, in_sem.at[len(names) - 1])
+    sum_ed = len(names)
     load("ed", ed_hbm.at[0], own_down)
+    both = down.at[pl.ds(0, half_fe + fd)]
+    names["ed"] = pltpu.make_async_copy(both, both, in_sem.at[sum_ed])
     load("dg", dg_hbm, dg)
     load("du", du_hbm, du)
-    load("dd", dd_hbm, down.at[pl.ds(2 * half_fe, fd)])
+    pltpu.make_async_copy(dd_hbm, down.at[pl.ds(2 * half_fe, fd)], in_sem.at[sum_ed]).start()
     load("og", og_hbm, out_gain)
     own = jnp.concatenate(own_rows_all, 0) * score_scale
     scores = jnp.concatenate(score_rows, 0) * score_scale
@@ -346,7 +349,7 @@
 
     lax.fori_loop(1, inner, send_mate, 0)
 
-    order = others + [zo]
+    order = [zo] + others
 
     def block_wait(ref, send_sem, recv_sem):
         return pltpu.make_async_remote_copy(
@@ -401,7 +404,7 @@
         rows = group * plane_rows
         planes = order[sum(groups[:c]) : sum(groups[: c + 1])]
         for k, p in enumerate(planes):
-            own_plane = c == chunks - 1 and k == group - 1
+            own_plane = c == 0 and k == group - 1
             count = inner - 1 if own_plane else inner
             block_wait(heads_all.at[pl.ds(0, count)], h_send, h_recv.at[p]).wait_recv()
             block_wait(rows_all.at[pl.ds(0, inner - 1)], r_send, r_plane.at[p]).wait_recv()
@@ -422,7 +425,7 @@
             value = (wide_rows[:rows, cols] - center) * inv * vector(attn_gain, cols)
             value = value.astype(BF16)
             mixed[:rows, cols] = value
-            if c == chunks - 1:
+            if c == 0:
                 own_mixed[:, cols] = value[rows - plane_rows :]
             gate = gate + row_sum(value.astype(F32) * vector(mix_gate, cols))
         blend = 1.0 / (1.0 + jnp.exp(-gate))
@@ -431,7 +434,7 @@
         weight = row_sum(jnp.where((c_lane == me) | (c_lane == me + n), tail, 0.0))
 
         if c == 0:
-            for name in ("eg", "eu", "ed", "dg", "du", "dd", "og"):
+            for name in ("eg", "ed", "dg", "du", "og"):
                 names[name].wait()
             for w in w_copies:
                 w.wait_recv()
@@ -448,7 +451,7 @@
                 block = part[k * plane_rows : (k + 1) * plane_rows].reshape(inner, seqs, tile)
                 sbuf[p, :, :, cols] = block.astype(BF16)
         for k, p in enumerate(planes):
-            if c == chunks - 1 and k == group - 1:
+            if c == 0 and k == group - 1:
                 plane_send(p, rbuf, s_plane, core, 1)
             else:
 
@@ -563,7 +566,7 @@
     inner = inner_size(n)
     outer = n // inner
     most = max(1, 128 // (inner * seqs))
-    groups = [1]
+    groups = [1] * min(outer, 2)
     while sum(groups) < outer:
         groups.append(min(most, outer - sum(groups)))
     top = max(groups) * inner * seqs
@@ -608,8 +611,8 @@
             VMEM(block, BF16),
             VMEM((outer, seqs, width), BF16),
             VMEM((outer, seqs, width), BF16),
-            dma((20,)),
-            dma((seqs,)),
+            dma((18,)),
+            dma,
             dma((3,)),
             dma((3,)),
             dma,

time: 25.4 us -> 25.2 us (level)
  Pallas kernels: 24.7 us -> 24.4 us
    pallas_call x1, Pallas kernels: 24.7 us -> 24.4 us  [on_device(): pl.pallas_call(functools.partial(kernel, n, tuple(groups)), out_shape=plt...]
where the time goes in v4:
time: 25.2 us; the launch traced here: 25 us
  Pallas kernels  24.4 us (97%)
  local copies, waits for them, and re-layouts  0.62 us (2%)
    pallas_call x1, Pallas kernels, on_device(): pl.pallas_call(functools.partial(kernel, n, tuple(groups)), out_shape=plt...  24.4 us
    unnamed x1, local copies, waits for them, and re-layouts  0.62 us

profile of v4, /device:TPU:0, one launch (start us, length us, event | category | flops | bytes accessed | tf_op | source)
XLA Modules:
  0.0 25.0 jit_solution(3527860505173251441)
XLA Ops:
  0.0 24.4 %shard_map.199 = bf16[8,2048]{1,0:T(8,128)(2,1)S(1)} custom-call(s32[8]{0:T(128)} %len_hbm.1, bf16[8,8,32]{2,1,0:T(8,128)(2,1)} %qr_hbm.1, bf16[8,32]{1,0:T(8,128)(2,1)} %rn_hbm.1, bf16[8,8,512]{2,1,0:T(8,128)(2,1)} %ql_hbm.1, bf16[8,512]{1,0:T(8,128)(2,1)} %ln_hbm.1, bf16[8,32,256]{2,1,0:T(8,128)(2,1)} %bitcast.5, bf16[8,256,512]{2,1,0:T(8,128)(2,1)} %cache_hbm.1, ...), custom_call_target="tpu_custom_call" | custom-call | tf_op jit(solution)/shard_map/pallas_call | solution.py:578
  24.4 0.6 %copy.23 = bf16[8,2048]{1,0:T(8,128)(2,1)} copy(bf16[8,2048]{1,0:T(8,128)(2,1)S(1)} %shard_map.199) | data formatting | bytes 65536

commit v5 on v4

--- a/solution.py
+++ b/solution.py
@@ -335,6 +335,12 @@
             device_id_type=MESH,
         )
 
+    def send_mate(d, carry):
+        head_copy(mate(d)).start()
+        return carry
+
+    lax.fori_loop(1, inner, send_mate, 0)
+
     for p in others:
 
         def send_line(i, carry):
@@ -343,11 +349,6 @@
 
         lax.fori_loop(0, inner, send_line, 0)
 
-    def send_mate(d, carry):
-        head_copy(mate(d)).start()
-        return carry
-
-    lax.fori_loop(1, inner, send_mate, 0)
 
     order = [zo] + others
 

time: 25.2 us -> 25 us (level)
  no operation moved by 1% of the time
where the time goes in v5:
time: 25 us; the launch traced here: 24.8 us
  Pallas kernels  24.2 us (97%)
  local copies, waits for them, and re-layouts  0.62 us (2%)
    pallas_call x1, Pallas kernels, on_device(): pl.pallas_call(functools.partial(kernel, n, tuple(groups)), out_shape=plt...  24.2 us
    unnamed x1, local copies, waits for them, and re-layouts  0.62 us

profile of v5, /device:TPU:0, one launch (start us, length us, event | category | flops | bytes accessed | tf_op | source)
XLA Modules:
  0.0 24.8 jit_solution(14186153205523986315)
XLA Ops:
  0.0 24.2 %shard_map.199 = bf16[8,2048]{1,0:T(8,128)(2,1)S(1)} custom-call(s32[8]{0:T(128)} %len_hbm.1, bf16[8,8,32]{2,1,0:T(8,128)(2,1)} %qr_hbm.1, bf16[8,32]{1,0:T(8,128)(2,1)} %rn_hbm.1, bf16[8,8,512]{2,1,0:T(8,128)(2,1)} %ql_hbm.1, bf16[8,512]{1,0:T(8,128)(2,1)} %ln_hbm.1, bf16[8,32,256]{2,1,0:T(8,128)(2,1)} %bitcast.5, bf16[8,256,512]{2,1,0:T(8,128)(2,1)} %cache_hbm.1, ...), custom_call_target="tpu_custom_call" | custom-call | tf_op jit(solution)/shard_map/pallas_call | solution.py:579
  24.2 0.6 %copy.23 = bf16[8,2048]{1,0:T(8,128)(2,1)} copy(bf16[8,2048]{1,0:T(8,128)(2,1)S(1)} %shard_map.199) | data formatting | bytes 65536
